TPU v7x, 32 devices: a whole 2x2x4 slice. The times are simulated.
32 devices in a mesh: sp: 8 (over z, y), tp: 4 (over x, core).
Axes of the slice: x: 2, y: 2, z: 4, core: 2. Of those that a mesh axis runs over, the one named last changes fastest.
Arguments:
- residual: bfloat16 [4096, 2048], P(('sp', 'tp')), may hold values from -6 to 6
- query_major: bfloat16 [4096, 1024], P('sp', 'tp'), may hold values from -160 to 160
- keys_major: bfloat16 [4096, 1024], P('sp', 'tp'), may hold values from -6.5 to 6.5
- values_major: bfloat16 [4096, 1024], P('sp', 'tp'), may hold values from -6 to 6
- query_minor: bfloat16 [4096, 512], P('sp', 'tp'), may hold values from -160 to 160
- keys_minor: bfloat16 [4096, 512], P('sp', 'tp'), may hold values from -6.5 to 6.5
- values_minor: bfloat16 [4096, 512], P('sp', 'tp'), may hold values from -6 to 6
- lambda_major: float32 [8], P('tp'), may hold values from 0.3 to 0.8
- lambda_minor: float32 [8], P('tp'), may hold values from 0.3 to 0.8
- gain_major: float32 [128], replicated, may hold values from 0.1 to 1.9
- gain_minor: float32 [64], replicated, may hold values from 0.1 to 1.9
- output_major: bfloat16 [1024, 2048], P('tp'), may hold values from -0.15625 to 0.15625
- output_minor: bfloat16 [512, 2048], P('tp'), may hold values from -0.15625 to 0.15625
- mixer_gain: float32 [2048], replicated, may hold values from 0.1 to 1.9
- up_weight: bfloat16 [2048, 8192], P('sp', 'tp'), may hold values from -0.125 to 0.125
- down_weight: bfloat16 [8192, 2048], P('tp', 'sp'), may hold values from -0.0625 to 0.0625
Outputs:
- layer_out: bfloat16 [4096, 2048], P(('sp', 'tp'))
All inputs are finite; a program needn't handle non-finite values.
Results may differ from a plain program's by a relative error of at most 0.018.
Values may be sent and summed in bfloat16 or wider, within the bound.
A program may use at most 128 MiB of HBM per device.

v0:
```python
import jax
import jax.numpy as jnp
from jax import lax
from jax.sharding import PartitionSpec as P

DK_MAJOR = 64
DK_MINOR = 32
SEGMENT = 64
EPSILON = 1e-06
NEGATIVE = -1e30


def swapped(value, axis, stride):
    mask = 2**stride
    pairs = [(source, source ^ mask) for source in range(lax.axis_size(axis))]
    return lax.ppermute(value, axis, pairs)


def to_wire(value):
    return lax.optimization_barrier(value.astype(jnp.bfloat16)).astype(jnp.float32)


def fresh(head_count, query_count, value_size):
    return (
        jnp.full((head_count, 2, query_count), NEGATIVE, jnp.float32),
        jnp.zeros((head_count, 2, query_count), jnp.float32),
        jnp.zeros((head_count, 2, query_count, value_size), jnp.float32),
    )


def fold_piece(carried, queries, key_rows, values, query_pos, key_size):
    head_count = key_rows.shape[1] // (2 * key_size)
    value_size = values.shape[1] // head_count
    query_count = queries.shape[0]
    block_len = min(key_rows.shape[0], query_count)
    query_heads = queries.reshape(query_count, head_count, 2, key_size)
    last_segment = query_pos[query_count - 1] // SEGMENT

    def visit(block_id, carried_in):
        key_first = block_id * block_len

        def update(running):
            peak_old, total_old, accum_old = running
            keys_block = lax.dynamic_slice_in_dim(key_rows, key_first, block_len, 0)
            keys_block = keys_block.reshape(block_len, head_count, 2, key_size)
            values_block = lax.dynamic_slice_in_dim(values, key_first, block_len, 0)
            values_block = values_block.reshape(block_len, head_count, value_size)
            key_pos = key_first + jnp.arange(block_len, dtype=jnp.int32)
            visible = key_pos[None, :] // SEGMENT <= query_pos[:, None] // SEGMENT
            scores = jnp.einsum(
                "qhmd,khmd->hmqk", query_heads, keys_block, preferred_element_type=jnp.float32
            ) * key_size ** (-0.5)
            scores = jnp.where(visible, scores, NEGATIVE)
            peak_new = jnp.maximum(peak_old, jnp.max(scores, axis=-1))
            weights = jnp.where(visible, jnp.exp(scores - peak_new[..., None]), 0.0)
            factor = jnp.exp(peak_old - peak_new)
            total_new = total_old * factor + jnp.sum(weights, axis=-1)
            accum_new = accum_old * factor[..., None] + jnp.einsum(
                "hmqk,khe->hmqe",
                weights.astype(jnp.bfloat16),
                values_block,
                preferred_element_type=jnp.float32,
            )
            return (peak_new, total_new, accum_new)

        def unchanged(running):
            return running

        block_segment = key_first // SEGMENT
        return lax.cond(block_segment <= last_segment, update, unchanged, carried_in)

    return lax.fori_loop(0, key_rows.shape[0] // block_len, visit, carried)


def finish(carried, lambdas, scaling):
    peak_unused, totals, accum = carried
    output = (
        accum[:, 0] / totals[:, 0, :, None]
        - lambdas[:, None, None] * accum[:, 1] / totals[:, 1, :, None]
    )
    output = (
        output * lax.rsqrt(jnp.mean(output * output, axis=-1, keepdims=True) + EPSILON) * scaling
    )
    head_count, query_count, value_size = output.shape
    return (
        jnp.transpose(output, (1, 0, 2))
        .reshape(query_count, head_count * value_size)
        .astype(jnp.bfloat16)
    )


def normalize(stream, scaling):
    normed = (
        stream * lax.rsqrt(jnp.mean(stream * stream, axis=-1, keepdims=True) + EPSILON) * scaling
    )
    return normed.astype(jnp.bfloat16)


def body(
    residual,
    query_major,
    keys_major,
    values_major,
    query_minor,
    keys_minor,
    values_minor,
    lambda_major,
    lambda_minor,
    gain_major,
    gain_minor,
    output_major,
    output_minor,
    mixer_gain,
    up_weight,
    down_weight,
):
    query_count = query_major.shape[0]
    half_rows = query_count // 2
    own_index = lax.axis_index("sp")
    sp_count = lax.axis_size("sp")
    sp_bits = sp_count.bit_length() - 1
    width_major = query_major.shape[1]
    early_pos = own_index * query_count + jnp.arange(half_rows, dtype=jnp.int32)
    early_major = query_major[:half_rows]
    early_minor = query_minor[:half_rows]
    late_queries = jnp.concatenate([query_major[half_rows:], query_minor[half_rows:]], axis=1)
    for bit_number in range(sp_bits):
        late_queries = swapped(late_queries, "sp", bit_number)
    late_major = late_queries[:, :width_major]
    late_minor = late_queries[:, width_major:]
    late_pos = (
        (sp_count - 1 - own_index) * query_count
        + half_rows
        + jnp.arange(half_rows, dtype=jnp.int32)
    )
    heads_major = keys_major.shape[1] // (2 * DK_MAJOR)
    heads_minor = keys_minor.shape[1] // (2 * DK_MINOR)
    size_major = values_major.shape[1] // heads_major
    size_minor = values_minor.shape[1] // heads_minor
    init_major = (
        fresh(heads_major, half_rows, size_major),
        fresh(heads_major, half_rows, size_major),
    )
    init_minor = (
        fresh(heads_minor, half_rows, size_minor),
        fresh(heads_minor, half_rows, size_minor),
    )
    pieces = (
        lax.all_gather(keys_major, "sp", axis=0, tiled=True),
        lax.all_gather(values_major, "sp", axis=0, tiled=True),
    )
    fold_pieces = (
        lax.all_gather(keys_minor, "sp", axis=0, tiled=True),
        lax.all_gather(values_minor, "sp", axis=0, tiled=True),
    )
    first_major = finish(
        fold_piece(init_major[0], early_major, pieces[0], pieces[1], early_pos, DK_MAJOR),
        lambda_major,
        gain_major,
    )
    first_minor = finish(
        fold_piece(init_minor[0], early_minor, fold_pieces[0], fold_pieces[1], early_pos, DK_MINOR),
        lambda_minor,
        gain_minor,
    )
    second_major = finish(
        fold_piece(init_major[1], late_major, pieces[0], pieces[1], late_pos, DK_MAJOR),
        lambda_major,
        gain_major,
    )
    second_minor = finish(
        fold_piece(init_minor[1], late_minor, fold_pieces[0], fold_pieces[1], late_pos, DK_MINOR),
        lambda_minor,
        gain_minor,
    )
    out_width = second_major.shape[1]
    late_out = jnp.concatenate([second_major, second_minor], axis=1)
    for bit_number in range(sp_bits):
        late_out = swapped(late_out, "sp", bit_number)
    second_major = late_out[:, :out_width]
    second_minor = late_out[:, out_width:]
    out_major = jnp.concatenate([first_major, second_major], axis=0)
    out_minor = jnp.concatenate([first_minor, second_minor], axis=0)
    partial_sum = jnp.dot(out_major, output_major, preferred_element_type=jnp.float32)
    partial_sum = partial_sum + jnp.dot(out_minor, output_minor, preferred_element_type=jnp.float32)
    mixed = lax.psum_scatter(
        to_wire(partial_sum).astype(jnp.bfloat16), "tp", scatter_dimension=0, tiled=True
    ).astype(jnp.float32)
    stream = residual.astype(jnp.float32) + mixed
    normed_all = lax.all_gather(normalize(stream, mixer_gain), "tp", axis=0, tiled=True)
    pre_act = jnp.dot(
        normed_all,
        lax.all_gather(up_weight, "sp", axis=0, tiled=True),
        preferred_element_type=jnp.float32,
    )
    hidden = jnp.square(jax.nn.relu(pre_act)).astype(jnp.bfloat16)
    down_full = lax.all_gather(down_weight, "sp", axis=1, tiled=True)
    down_sum = lax.psum_scatter(
        to_wire(jnp.dot(hidden, down_full, preferred_element_type=jnp.float32)).astype(
            jnp.bfloat16
        ),
        "tp",
        scatter_dimension=0,
        tiled=True,
    ).astype(jnp.float32)
    return (stream + down_sum).astype(jnp.bfloat16)


def solution(mesh):
    return jax.shard_map(
        body,
        mesh=mesh,
        in_specs=(
            P(("sp", "tp"), None),
            P("sp", "tp"),
            P("sp", "tp"),
            P("sp", "tp"),
            P("sp", "tp"),
            P("sp", "tp"),
            P("sp", "tp"),
            P("tp"),
            P("tp"),
            P(),
            P(),
            P("tp", None),
            P("tp", None),
            P(),
            P("sp", "tp"),
            P("tp", "sp"),
        ),
        out_specs=P(("sp", "tp"), None),
        check_vma=False,
    )
```

profile of v0, /device:TPU:0, one launch (start us, length us, event | category | flops | bytes accessed | tf_op | source)
XLA Modules:
  0.0 631.5 jit_solution(7971657574266542645)
XLA Ops:
  6.5 1.7 copy.48
  8.4 1.7 copy.50
  10.1 1.8 copy.42
  12.0 1.8 copy.40
  15.8 3.1 collective-permute-start
  18.8 6.3 collective-permute-done
  25.1 1.8 collective-permute-start.1
  26.9 4.9 collective-permute-done.1
  31.9 3.2 collective-permute-start.2
  41.7 3.5 collective-permute-done.2
  45.5 9.6 %all-gather.12.cloned.1.call-done = bf16[4096,128]{0,1:T(8,128)(2,1)} async-done(((bf16[512,128]{0,1:T(8,128)(2,1)}), bf16[4096,128]{0,1:T(8,128)(2,1)}) %all-gather.12.cloned.1.call-update) | async-done | bytes 1048592 | tf_op jit(solution)/shard_map/all_gather | solution.py:153
  55.0 42.4 %all-gather.14.cloned.1.call-done = bf16[4096,128]{0,1:T(8,128)(2,1)} async-done(((bf16[512,128]{0,1:T(8,128)(2,1)}), bf16[4096,128]{0,1:T(8,128)(2,1)}) %all-gather.14.cloned.1.call-update) | async-done | bytes 1048592 | tf_op jit(solution)/shard_map/all_gather | solution.py:154
  97.5 33.4 %while.82 = (s32[]{:T(128)}, f32[2,2,256]{2,1,0:T(2,128)S(1)}, f32[2,2,256]{2,1,0:T(2,128)S(1)}, f32[2,2,256,64]{2,3,1,0:T(8,128)S(1)}, s32[]{:T(128)}, /*index=...) while((s32[]{:T(128)}, f32[2,2,256]{2,1,0:T(2,128)S(1)}, ...), condition=%wide.region_19.20_spmd.clone, body=%wide.region_14.19_spmd.clone.sunk | while | flops 52897816 | bytes 4463083 | solution.py:72
  97.5 2.0 conditional.14
  99.6 2.0 conditional.14
  101.7 2.0 conditional.14
  103.8 2.0 conditional.14
  105.9 2.0 conditional.14
  108.0 2.0 conditional.14
  110.1 2.0 conditional.14
  112.2 2.0 conditional.14
  114.3 2.0 conditional.14
  116.3 2.0 conditional.14
  118.4 2.0 conditional.14
  120.5 2.0 conditional.14
  122.6 2.0 conditional.14
  124.7 2.0 conditional.14
  126.8 2.0 conditional.14
  128.9 2.0 conditional.14
  131.0 3.3 while.83
  131.1 2.0 conditional.15
  134.6 14.2 %all-gather.10.cloned.1.call-done = bf16[4096,256]{0,1:T(8,128)(2,1)} async-done(((bf16[512,256]{0,1:T(8,128)(2,1)}), bf16[4096,256]{0,1:T(8,128)(2,1)}) %all-gather.10.cloned.1.call-update) | async-done | bytes 2097168 | tf_op jit(solution)/shard_map/all_gather | solution.py:150
  148.8 50.5 %all-gather.8.cloned.1.call-done = bf16[4096,256]{0,1:T(8,128)(2,1)} async-done(((bf16[512,256]{0,1:T(8,128)(2,1)}), bf16[4096,256]{0,1:T(8,128)(2,1)}) %all-gather.8.cloned.1.call-update) | async-done | bytes 2097168 | tf_op jit(solution)/shard_map/all_gather | solution.py:149
  199.4 38.5 %while.81 = (s32[]{:T(128)}, f32[2,2,256]{2,1,0:T(2,128)S(1)}, f32[2,2,256]{2,1,0:T(2,128)S(1)}, f32[2,2,256,128]{3,2,1,0:T(8,128)S(1)}, s32[]{:T(128)}, /*index...) while((s32[]{:T(128)}, f32[2,2,256]{2,1,0:T(2,128)S(1)}, ...), condition=%wide.region_12.13_spmd.clone, body=%wide.region_7.12_spmd.clone.sunk | while | flops 103360528 | bytes 5446123 | solution.py:72
  199.4 2.3 conditional.13
  201.8 2.3 conditional.13
  204.2 2.3 conditional.13
  206.6 2.3 conditional.13
  209.1 2.3 conditional.13
  211.5 2.3 conditional.13
  213.9 2.3 conditional.13
  216.3 2.3 conditional.13
  218.7 2.3 conditional.13
  221.1 2.3 conditional.13
  223.5 2.3 conditional.13
  225.9 2.3 conditional.13
  228.3 2.3 conditional.13
  230.7 2.3 conditional.13
  233.1 2.3 conditional.13
  235.5 2.3 conditional.13
  238.0 3.6 while.80
  238.0 2.4 conditional.12
  245.2 5.0 collective-permute-done.3
  250.2 5.7 collective-permute-done.4
  256.9 8.6 %collective-permute-done.5 = bf16[256,384]{0,1:T(8,128)(2,1)S(1)} collective-permute-done((bf16[256,384]{0,1:T(8,128)(2,1)S(1)}, bf16[256,384]{0,1:T(8,128)(2,1)S(1)}, u32[]{:S(2)}, u32[]{:S(2)}) %collective-permute-start.5) | collective-permute-done | bytes 196640 | tf_op jit(solution)/shard_map/ppermute | solution.py:16
  266.2 2.1 add_convert_fusion
  268.4 30.5 %reduce-scatter.3.cloned.1.call-done = bf16[128,2048]{1,0:T(8,128)(2,1)} async-done(((bf16[512,2048]{1,0:T(8,128)(2,1)}), bf16[128,2048]{1,0:T(8,128)(2,1)}) %reduce-scatter.3.cloned.1.call-update) | async-done | bytes 524304 | tf_op jit(solution)/shard_map/reduce_scatter | solution.py:186
  300.2 2.0 multiply_convert_fusion.1
  304.0 21.0 %all-gather.16.cloned.1.call-done = bf16[512,2048]{1,0:T(8,128)(2,1)} async-done(((bf16[128,2048]{1,0:T(8,128)(2,1)}), bf16[512,2048]{1,0:T(8,128)(2,1)}) %all-gather.16.cloned.1.call-update) | async-done | bytes 2097168 | tf_op jit(solution)/shard_map/all_gather | solution.py:190
  325.0 126.6 %all-gather.18.cloned.1.call-done = bf16[2048,2048]{1,0:T(8,128)(2,1)} async-done(((bf16[256,2048]{1,0:T(8,128)(2,1)}), bf16[2048,2048]{1,0:T(8,128)(2,1)}) %all-gather.18.cloned.1.call-update) | async-done | bytes 8388624 | tf_op jit(solution)/shard_map/all_gather | solution.py:193
  451.6 125.2 %all-gather.20.cloned.1.call-done = bf16[2048,2048]{1,0:T(8,128)(2,1)} async-done(((bf16[2048,256]{1,0:T(8,128)(2,1)}), bf16[2048,2048]{1,0:T(8,128)(2,1)}) %all-gather.20.cloned.1.call-update) | async-done | bytes 8388624 | tf_op jit(solution)/shard_map/all_gather | solution.py:197
  576.8 16.5 %convolution_convert_fusion = bf16[512,2048]{1,0:T(8,128)(2,1)} fusion(bf16[2048,2048]{1,0:T(8,128)(2,1)} %all-gather.20.cloned.1.call-done, bf16[512,2048]{1,0:T(8,128)(2,1)} %all-gather.16.cloned.1.call-done, bf16[2048,2048]{1,0:T(8,128)(2,1)} %all-gather.18.cloned.1.call-done), kind=kOutput, calls=%fused_computation.102 | convolution fusion | flops 8594128896 | bytes 20971520 | tf_op jit(solution)/shard_map/dot_general | solution.py:199
  593.4 29.5 %reduce-scatter.5.cloned.1.call-done = bf16[128,2048]{1,0:T(8,128)(2,1)} async-done(((bf16[512,2048]{1,0:T(8,128)(2,1)}), bf16[128,2048]{1,0:T(8,128)(2,1)}) %reduce-scatter.5.cloned.1.call-update) | async-done | bytes 524304 | tf_op jit(solution)/shard_map/reduce_scatter | solution.py:198
  622.9 2.1 add_convert_fusion.1
  (484 shorter events, 85.2 us)
Async XLA Ops:
  6.5 259.7 %copy-start = (bf16[256,2048]{1,0:T(8,128)(2,1)S(1)}, bf16[256,2048]{1,0:T(8,128)(2,1)}, u32[]{:S(2)}) copy-start(bf16[256,2048]{1,0:T(8,128)(2,1)} %param.43) | copy-start | bytes 3145732
  6.5 48.5 %all-gather.12.cloned.1.call-start = ((), (), s32[]{:S(2)}) async-start(), calls=%async_computation.4 | async-start | bytes 1179648 | tf_op jit(solution)/shard_map/all_gather | solution.py:153
  8.3 89.1 %all-gather.14.cloned.1.call-start = ((), (), s32[]{:S(2)}) async-start(), calls=%async_computation.5 | async-start | bytes 1179648 | tf_op jit(solution)/shard_map/all_gather | solution.py:154
  10.1 138.8 %all-gather.10.cloned.1.call-start = ((), (), s32[]{:S(2)}) async-start(), calls=%async_computation.3 | async-start | bytes 2359296 | tf_op jit(solution)/shard_map/all_gather | solution.py:150
  11.9 187.4 %all-gather.8.cloned.1.call-start = ((), (), s32[]{:S(2)}) async-start(), calls=%async_computation.2 | async-start | bytes 2359296 | tf_op jit(solution)/shard_map/all_gather | solution.py:149
  13.8 285.1 %reduce-scatter.3.cloned.1.call-start = ((), (), s32[]{:S(2)}) async-start(), calls=%async_computation.6 | async-start | bytes 2621440 | tf_op jit(solution)/shard_map/reduce_scatter | solution.py:186
  15.8 9.4 %collective-permute-start = (bf16[256,384]{1,0:T(8,128)(2,1)S(1)}, bf16[256,384]{1,0:T(8,128)(2,1)S(1)}, u32[]{:S(2)}, u32[]{:S(2)}) collective-permute-start(bf16[256,384]{1,0:T(8,128)(2,1)S(1)} %pad_maximum_fusion), channel_id=1, source_target_pairs={{0,4},{4,0},{8,12},{12,8},{16,20},{20,16},{24,28},{28,24},{1,5},{5... | collective-permute-start | bytes 589832 | tf_op jit(solution)/shard_map/ppermute | solution.py:16
  25.1 6.7 %collective-permute-start.1 = (bf16[256,384]{1,0:T(8,128)(2,1)S(1)}, bf16[256,384]{1,0:T(8,128)(2,1)S(1)}, u32[]{:S(2)}, u32[]{:S(2)}) collective-permute-start(bf16[256,384]{1,0:T(8,128)(2,1)S(1)} %collective-permute-done), channel_id=1, source_target_pairs={{0,8},{4,12},{8,0},{12,4},{16,24},{20,28},{24,16},{28,20},{1,9},{5... | collective-permute-start | bytes 589832 | tf_op jit(solution)/shard_map/ppermute | solution.py:16
  31.9 13.4 %collective-permute-start.2 = (bf16[256,384]{1,0:T(8,128)(2,1)S(1)}, bf16[256,384]{1,0:T(8,128)(2,1)S(1)}, u32[]{:S(2)}, u32[]{:S(2)}) collective-permute-start(bf16[256,384]{1,0:T(8,128)(2,1)S(1)} %collective-permute-done.1), channel_id=1, source_target_pairs={{0,16},{4,20},{8,24},{12,28},{16,0},{20,4},{24,8},{28,12},{1,17},{... | collective-permute-start | bytes 589832 | tf_op jit(solution)/shard_map/ppermute | solution.py:16
  131.0 3.4 copy-start.6
  131.0 3.5 copy-start.5
  241.6 23.9 %copy-start.3 = (bf16[128,2048]{1,0:T(8,128)(2,1)S(1)}, bf16[128,2048]{1,0:T(8,128)(2,1)}, u32[]{:S(2)}) copy-start(bf16[128,2048]{1,0:T(8,128)(2,1)} %param.44) | copy-start | bytes 1572868
  243.7 6.5 %collective-permute-start.3 = (bf16[256,384]{0,1:T(8,128)(2,1)S(1)}, bf16[256,384]{0,1:T(8,128)(2,1)S(1)}, u32[]{:S(2)}, u32[]{:S(2)}) collective-permute-start(bf16[256,384]{0,1:T(8,128)(2,1)S(1)} %pad_maximum_fusion.1), channel_id=1, source_target_pairs={{0,4},{4,0},{8,12},{12,8},{16,20},{20,16},{24,28},{28,24},{1,5},{5... | collective-permute-start | bytes 589832 | tf_op jit(solution)/shard_map/ppermute | solution.py:16
  250.2 5.7 collective-permute-start.4
  255.9 9.6 %collective-permute-start.5 = (bf16[256,384]{0,1:T(8,128)(2,1)S(1)}, bf16[256,384]{0,1:T(8,128)(2,1)S(1)}, u32[]{:S(2)}, u32[]{:S(2)}) collective-permute-start(bf16[256,384]{0,1:T(8,128)(2,1)S(1)} %collective-permute-done.4), channel_id=1, source_target_pairs={{0,16},{4,20},{8,24},{12,28},{16,0},{20,4},{24,8},{28,12},{1,17},{... | collective-permute-start | bytes 589832 | tf_op jit(solution)/shard_map/ppermute | solution.py:16
  266.2 32.7 %copy-start.1 = (bf16[128,2048]{1,0:T(8,128)(2,1)S(1)}, bf16[128,2048]{1,0:T(8,128)(2,1)}, u32[]{:S(2)}) copy-start(bf16[128,2048]{1,0:T(8,128)(2,1)} %param.32) | copy-start | bytes 1572868
  266.2 34.0 %copy-start.4 = (f32[2048]{0:T(1024)S(1)}, f32[2048]{0:T(1024)}, u32[]{:S(2)}) copy-start(f32[2048]{0:T(1024)} %param.45) | copy-start | bytes 24580
  268.4 56.6 %all-gather.16.cloned.1.call-start = ((), (), s32[]{:S(2)}) async-start(), calls=%async_computation.7 | async-start | bytes 2621440 | tf_op jit(solution)/shard_map/all_gather | solution.py:190
  302.3 149.4 %all-gather.18.cloned.1.call-start = ((), (), s32[]{:S(2)}) async-start(), calls=%async_computation.8 | async-start | bytes 9437184 | tf_op jit(solution)/shard_map/all_gather | solution.py:193
  303.0 273.8 %all-gather.20.cloned.1.call-start = ((), (), s32[]{:S(2)}) async-start(), calls=%async_computation.9 | async-start | bytes 9437184 | tf_op jit(solution)/shard_map/all_gather | solution.py:197
  303.8 319.1 %copy-start.2 = (bf16[128,2048]{1,0:T(8,128)(2,1)S(1)}, bf16[128,2048]{1,0:T(8,128)(2,1)}, u32[]{:S(2)}) copy-start(bf16[128,2048]{1,0:T(8,128)(2,1)} %reduce-scatter.3.cloned.1.call-done) | copy-start | bytes 1572868
  303.8 319.1 %reduce-scatter.5.cloned.1.call-start = ((), (), s32[]{:S(2)}) async-start(), calls=%async_computation.10 | async-start | bytes 2621440 | tf_op jit(solution)/shard_map/reduce_scatter | solution.py:198
Sparse Core Ops, SparseCore 0:
  9.4 45.6 all-gather.11
  57.1 40.3 all-gather.13
  99.5 49.2 all-gather.9
  150.7 48.5 all-gather.7
  268.5 30.3 reduce-scatter.2
  302.4 22.5 all-gather.15
  327.1 124.4 all-gather.17
  453.7 123.1 all-gather.19
  593.5 29.3 reduce-scatter.4
where the time goes:
time: 633 us; the launch traced here: 631 us
  waiting for transfers between devices  485 us (77%)
  matrix products  47.3 us (7%)
  local copies, waits for them, and re-layouts  43.4 us (7%)
  other arithmetic  19.2 us (3%)
  between operations  18.8 us (3%)
  starting transfers between devices  11 us (2%)
  loops' own time  6.78 us (1%)
    all_gather x1, waiting for transfers between devices, body(): lax.all_gather(up_weight, 'sp', axis=0, tiled=True)  127 us
    all_gather x1, waiting for transfers between devices, body(): down_full = lax.all_gather(down_weight, 'sp', axis=1, tiled=True)  125 us
    all_gather x1, waiting for transfers between devices, body(): lax.all_gather(keys_major, 'sp', axis=0, tiled=True)  50.5 us
    all_gather x1, waiting for transfers between devices, body(): lax.all_gather(values_minor, 'sp', axis=0, tiled=True)  42.4 us
    ppermute x6, waiting for transfers between devices, swapped(): return lax.ppermute(value, axis, pairs)  34 us
    dynamic_slice x34, local copies, waits for them, and re-layouts, update(): values_block = lax.dynamic_slice_in_dim(values, key_first, block_len, 0)  32 us
    reduce_scatter x1, waiting for transfers between devices, body(): lax.psum_scatter(to_wire(partial_sum).astype(jnp.bfloat16), 'tp', scatter...  30.5 us
    reduce_scatter x1, waiting for transfers between devices, body(): lax.psum_scatter(to_wire(jnp.dot(hidden, down_full, preferred_element_typ...  29.5 us
  transfers between devices with their start and end apart: 15, of which 15 were waited for; matrix products, arithmetic and copies ran while one was open for 7% of the time, Pallas kernels for 0%

commit v1 on v0

--- a/solution.py
+++ b/solution.py
@@ -151,7 +151,9 @@
     )
     fold_pieces = (
         lax.all_gather(keys_minor, "sp", axis=0, tiled=True),
-        lax.all_gather(values_minor, "sp", axis=0, tiled=True),
+        jnp.concatenate(
+            lax.all_to_all(jnp.stack([values_minor] * lax.axis_size("sp")), "sp", 0, 0), axis=0
+        ),
     )
     first_major = finish(
         fold_piece(init_major[0], early_major, pieces[0], pieces[1], early_pos, DK_MAJOR),

time: 633 us -> 604 us (0.954)
  waiting for transfers between devices: 485 us -> 449 us
  starting transfers between devices: 11 us -> 19.8 us
    all_gather x1 -> x0, waiting for transfers between devices: 42.4 us -> none  [body(): lax.all_gather(values_minor, 'sp', axis=0, tiled=True)]
    all_gather x1, waiting for transfers between devices: 14.2 us -> 50.6 us  [body(): lax.all_gather(values_major, 'sp', axis=0, tiled=True)]
    all_gather x1, waiting for transfers between devices: 50.5 us -> 15.3 us  [body(): lax.all_gather(keys_major, 'sp', axis=0, tiled=True)]
    ppermute x6, waiting for transfers between devices: 34 us -> 46.8 us  [swapped(): return lax.ppermute(value, axis, pairs)]
    all_gather x1, waiting for transfers between devices: 9.58 us -> 1.74 us  [body(): lax.all_gather(keys_minor, 'sp', axis=0, tiled=True)]
    all_to_all x0 -> x1, starting transfers between devices: none -> 7.31 us  [body(): lax.all_to_all(jnp.stack([values_minor] * lax.axis_size('sp')), 'sp', 0, 0)]
  transfers between devices with their start and end apart: 15 -> 15, of which waited for: 15 -> 14; matrix products, arithmetic and copies ran while one was open for 7% -> 7% of each run, Pallas kernels for 0% -> 0%
where the time goes in v1:
time: 604 us; the launch traced here: 602 us
  waiting for transfers between devices  449 us (74%)
  matrix products  47.3 us (8%)
  local copies, waits for them, and re-layouts  43.1 us (7%)
  starting transfers between devices  19.8 us (3%)
  between operations  18.8 us (3%)
  other arithmetic  17.9 us (3%)
  loops' own time  6.78 us (1%)
    all_gather x1, waiting for transfers between devices, body(): lax.all_gather(up_weight, 'sp', axis=0, tiled=True)  126 us
    all_gather x1, waiting for transfers between devices, body(): down_full = lax.all_gather(down_weight, 'sp', axis=1, tiled=True)  125 us
    all_gather x1, waiting for transfers between devices, body(): lax.all_gather(values_major, 'sp', axis=0, tiled=True)  50.6 us
    ppermute x6, waiting for transfers between devices, swapped(): return lax.ppermute(value, axis, pairs)  46.8 us
    dynamic_slice x34, local copies, waits for them, and re-layouts, update(): values_block = lax.dynamic_slice_in_dim(values, key_first, block_len, 0)  32 us
    reduce_scatter x1, waiting for transfers between devices, body(): lax.psum_scatter(to_wire(partial_sum).astype(jnp.bfloat16), 'tp', scatter...  30.4 us
    reduce_scatter x1, waiting for transfers between devices, body(): lax.psum_scatter(to_wire(jnp.dot(hidden, down_full, preferred_element_typ...  29.5 us
    all_gather x1, waiting for transfers between devices, body(): lax.all_gather(normalize(stream, mixer_gain), 'tp', axis=0, tiled=True)  21.2 us
  transfers between devices with their start and end apart: 15, of which 14 were waited for; matrix products, arithmetic and copies ran while one was open for 7% of the time, Pallas kernels for 0%

profile of v1, /device:TPU:0, one launch (start us, length us, event | category | flops | bytes accessed | tf_op | source)
XLA Modules:
  0.0 602.1 jit_solution(16024482495308305158)
XLA Ops:
  6.6 1.8 copy.90
  8.4 1.8 copy.82
  12.3 7.3 %all-to-all-start = ((bf16[8,512,128]{1,2,0:T(8,128)(2,1)}), bf16[8,512,128]{1,2,0:T(8,128)(2,1)S(1)}, u32[]{:S(2)}, u32[]{:S(2)}) async-start(bf16[8,512,128]{1,2,0:T(8,128)(2,1)} %stack.2), calls=%async_computation | async-start | bytes 2097152 | tf_op jit(solution)/shard_map/all_to_all | solution.py:155
  20.7 2.0 collective-permute-start
  22.8 12.8 %collective-permute-done = bf16[256,384]{1,0:T(8,128)(2,1)S(1)} collective-permute-done((bf16[256,384]{1,0:T(8,128)(2,1)S(1)}, bf16[256,384]{1,0:T(8,128)(2,1)S(1)}, u32[]{:S(2)}, u32[]{:S(2)}) %collective-permute-start) | collective-permute-done | bytes 196640 | tf_op jit(solution)/shard_map/ppermute | solution.py:16
  35.6 9.5 %collective-permute-done.1 = bf16[256,384]{1,0:T(8,128)(2,1)S(1)} collective-permute-done((bf16[256,384]{1,0:T(8,128)(2,1)S(1)}, bf16[256,384]{1,0:T(8,128)(2,1)S(1)}, u32[]{:S(2)}, u32[]{:S(2)}) %collective-permute-start.1) | collective-permute-done | bytes 196640 | tf_op jit(solution)/shard_map/ppermute | solution.py:16
  45.1 7.4 %collective-permute-start.2 = (bf16[256,384]{1,0:T(8,128)(2,1)S(1)}, bf16[256,384]{1,0:T(8,128)(2,1)S(1)}, u32[]{:S(2)}, u32[]{:S(2)}) collective-permute-start(bf16[256,384]{1,0:T(8,128)(2,1)S(1)} %collective-permute-done.1), channel_id=1, source_target_pairs={{0,16},{4,20},{8,24},{12,28},{16,0},{20,4},{24,8},{28,12},{1,17},{... | collective-permute-start | bytes 589832 | tf_op jit(solution)/shard_map/ppermute | solution.py:16
  58.8 5.2 collective-permute-done.2
  64.9 1.3 copy.94
  66.2 1.7 all-gather.11.cloned.1.call-done
  68.0 33.4 %while.82 = (s32[]{:T(128)}, f32[2,2,256]{2,1,0:T(2,128)S(1)}, f32[2,2,256]{2,1,0:T(2,128)S(1)}, f32[2,2,256,64]{2,3,1,0:T(8,128)S(1)}, s32[]{:T(128)}, /*index=...) while((s32[]{:T(128)}, f32[2,2,256]{2,1,0:T(2,128)S(1)}, ...), condition=%wide.region_19.20_spmd.clone, body=%wide.region_14.19_spmd.clone.sunk | while | flops 52897816 | bytes 4463083 | solution.py:72
  68.1 2.0 conditional.14
  70.2 2.0 conditional.14
  72.3 2.0 conditional.14
  74.3 2.0 conditional.14
  76.4 2.0 conditional.14
  78.5 2.0 conditional.14
  80.6 2.0 conditional.14
  82.7 2.0 conditional.14
  84.8 2.0 conditional.14
  86.9 2.0 conditional.14
  89.0 2.0 conditional.14
  91.0 2.0 conditional.14
  93.1 2.0 conditional.14
  95.2 2.0 conditional.14
  97.3 2.0 conditional.14
  99.4 2.0 conditional.14
  101.5 3.3 while.83
  101.6 2.0 conditional.15
  105.1 15.3 %all-gather.7.cloned.1.call-done = bf16[4096,256]{0,1:T(8,128)(2,1)} async-done(((bf16[512,256]{0,1:T(8,128)(2,1)}), bf16[4096,256]{0,1:T(8,128)(2,1)}) %all-gather.7.cloned.1.call-update) | async-done | bytes 2097168 | tf_op jit(solution)/shard_map/all_gather | solution.py:149
  120.5 50.6 %all-gather.9.cloned.1.call-done = bf16[4096,256]{0,1:T(8,128)(2,1)} async-done(((bf16[512,256]{0,1:T(8,128)(2,1)}), bf16[4096,256]{0,1:T(8,128)(2,1)}) %all-gather.9.cloned.1.call-update) | async-done | bytes 2097168 | tf_op jit(solution)/shard_map/all_gather | solution.py:150
  171.1 38.5 %while.81 = (s32[]{:T(128)}, f32[2,2,256]{2,1,0:T(2,128)S(1)}, f32[2,2,256]{2,1,0:T(2,128)S(1)}, f32[2,2,256,128]{3,2,1,0:T(8,128)S(1)}, s32[]{:T(128)}, /*index...) while((s32[]{:T(128)}, f32[2,2,256]{2,1,0:T(2,128)S(1)}, ...), condition=%wide.region_12.13_spmd.clone, body=%wide.region_7.12_spmd.clone.sunk | while | flops 103360528 | bytes 5446123 | solution.py:72
  171.2 2.3 conditional.13
  173.6 2.3 conditional.13
  176.0 2.3 conditional.13
  178.4 2.3 conditional.13
  180.8 2.3 conditional.13
  183.2 2.3 conditional.13
  185.6 2.3 conditional.13
  188.1 2.3 conditional.13
  190.5 2.3 conditional.13
  192.9 2.3 conditional.13
  195.3 2.3 conditional.13
  197.7 2.3 conditional.13
  200.1 2.3 conditional.13
  202.5 2.3 conditional.13
  204.9 2.3 conditional.13
  207.3 2.3 conditional.13
  209.8 3.6 while.80
  209.8 2.3 conditional.12
  214.2 1.5 collective-permute-start.3
  215.7 5.0 collective-permute-done.3
  220.7 5.7 collective-permute-done.4
  227.4 8.6 %collective-permute-done.5 = bf16[256,384]{0,1:T(8,128)(2,1)S(1)} collective-permute-done((bf16[256,384]{0,1:T(8,128)(2,1)S(1)}, bf16[256,384]{0,1:T(8,128)(2,1)S(1)}, u32[]{:S(2)}, u32[]{:S(2)}) %collective-permute-start.5) | collective-permute-done | bytes 196640 | tf_op jit(solution)/shard_map/ppermute | solution.py:16
  236.8 2.1 add_convert_fusion
  238.9 30.4 %reduce-scatter.3.cloned.1.call-done = bf16[128,2048]{1,0:T(8,128)(2,1)} async-done(((bf16[512,2048]{1,0:T(8,128)(2,1)}), bf16[128,2048]{1,0:T(8,128)(2,1)}) %reduce-scatter.3.cloned.1.call-update) | async-done | bytes 524304 | tf_op jit(solution)/shard_map/reduce_scatter | solution.py:188
  269.4 1.3 multiply_reduce_fusion
  270.7 2.0 multiply_convert_fusion.1
  274.3 21.2 %all-gather.13.cloned.1.call-done = bf16[512,2048]{1,0:T(8,128)(2,1)} async-done(((bf16[128,2048]{1,0:T(8,128)(2,1)}), bf16[512,2048]{1,0:T(8,128)(2,1)}) %all-gather.13.cloned.1.call-update) | async-done | bytes 2097168 | tf_op jit(solution)/shard_map/all_gather | solution.py:192
  295.5 126.5 %all-gather.15.cloned.1.call-done = bf16[2048,2048]{1,0:T(8,128)(2,1)} async-done(((bf16[256,2048]{1,0:T(8,128)(2,1)}), bf16[2048,2048]{1,0:T(8,128)(2,1)}) %all-gather.15.cloned.1.call-update) | async-done | bytes 8388624 | tf_op jit(solution)/shard_map/all_gather | solution.py:195
  422.0 125.2 %all-gather.17.cloned.1.call-done = bf16[2048,2048]{1,0:T(8,128)(2,1)} async-done(((bf16[2048,256]{1,0:T(8,128)(2,1)}), bf16[2048,2048]{1,0:T(8,128)(2,1)}) %all-gather.17.cloned.1.call-update) | async-done | bytes 8388624 | tf_op jit(solution)/shard_map/all_gather | solution.py:199
  547.2 16.5 %convolution_convert_fusion = bf16[512,2048]{1,0:T(8,128)(2,1)} fusion(bf16[2048,2048]{1,0:T(8,128)(2,1)} %all-gather.17.cloned.1.call-done, bf16[512,2048]{1,0:T(8,128)(2,1)} %all-gather.13.cloned.1.call-done, bf16[2048,2048]{1,0:T(8,128)(2,1)} %all-gather.15.cloned.1.call-done), kind=kOutput, calls=%fused_computation.102 | convolution fusion | flops 8594128896 | bytes 20971520 | tf_op jit(solution)/shard_map/dot_general | solution.py:201
  563.7 29.5 %reduce-scatter.5.cloned.1.call-done = bf16[128,2048]{1,0:T(8,128)(2,1)} async-done(((bf16[512,2048]{1,0:T(8,128)(2,1)}), bf16[128,2048]{1,0:T(8,128)(2,1)}) %reduce-scatter.5.cloned.1.call-update) | async-done | bytes 524304 | tf_op jit(solution)/shard_map/reduce_scatter | solution.py:200
  593.2 2.1 add_convert_fusion.1
  (496 shorter events, 82.7 us)
Async XLA Ops:
  6.5 230.2 %copy-start = (bf16[256,2048]{1,0:T(8,128)(2,1)S(1)}, bf16[256,2048]{1,0:T(8,128)(2,1)}, u32[]{:S(2)}) copy-start(bf16[256,2048]{1,0:T(8,128)(2,1)} %param.43) | copy-start | bytes 3145732
  6.5 13.2 %copy-start.4 = (bf16[512,256]{1,0:T(8,128)(2,1)S(1)}, bf16[512,256]{1,0:T(8,128)(2,1)}, u32[]{:S(2)}) copy-start(bf16[512,256]{1,0:T(8,128)(2,1)} %param.35) | copy-start | bytes 786436
  6.5 14.1 %copy-start.6 = (bf16[512,128]{1,0:T(8,128)(2,1)S(1)}, bf16[512,128]{1,0:T(8,128)(2,1)}, u32[]{:S(2)}) copy-start(bf16[512,128]{1,0:T(8,128)(2,1)} %param.36) | copy-start | bytes 393220
  6.5 14.1 %copy-start.5 = (bf16[512,256]{1,0:T(8,128)(2,1)S(1)}, bf16[512,256]{1,0:T(8,128)(2,1)}, u32[]{:S(2)}) copy-start(bf16[512,256]{1,0:T(8,128)(2,1)} %param.33) | copy-start | bytes 786436
  6.5 61.4 %all-gather.11.cloned.1.call-start = ((), (), s32[]{:S(2)}) async-start(), calls=%async_computation.5 | async-start | bytes 1179648 | tf_op jit(solution)/shard_map/all_gather | solution.py:153
  8.4 112.1 %all-gather.7.cloned.1.call-start = ((), (), s32[]{:S(2)}) async-start(), calls=%async_computation.3 | async-start | bytes 2359296 | tf_op jit(solution)/shard_map/all_gather | solution.py:149
  12.3 51.9 %all-to-all-start = ((bf16[8,512,128]{1,2,0:T(8,128)(2,1)}), bf16[8,512,128]{1,2,0:T(8,128)(2,1)S(1)}, u32[]{:S(2)}, u32[]{:S(2)}) async-start(bf16[8,512,128]{1,2,0:T(8,128)(2,1)} %stack.2), calls=%async_computation | async-start | bytes 2097152 | tf_op jit(solution)/shard_map/all_to_all | solution.py:155
  19.7 151.4 %all-gather.9.cloned.1.call-start = ((), (), s32[]{:S(2)}) async-start(), calls=%async_computation.4 | async-start | bytes 2359296 | tf_op jit(solution)/shard_map/all_gather | solution.py:150
  20.6 248.8 %reduce-scatter.3.cloned.1.call-start = ((), (), s32[]{:S(2)}) async-start(), calls=%async_computation.6 | async-start | bytes 2621440 | tf_op jit(solution)/shard_map/reduce_scatter | solution.py:188
  20.7 14.8 %collective-permute-start = (bf16[256,384]{1,0:T(8,128)(2,1)S(1)}, bf16[256,384]{1,0:T(8,128)(2,1)S(1)}, u32[]{:S(2)}, u32[]{:S(2)}) collective-permute-start(bf16[256,384]{1,0:T(8,128)(2,1)S(1)} %pad_maximum_fusion), channel_id=1, source_target_pairs={{0,4},{4,0},{8,12},{12,8},{16,20},{20,16},{24,28},{28,24},{1,5},{5... | collective-permute-start | bytes 589832 | tf_op jit(solution)/shard_map/ppermute | solution.py:16
  35.5 9.6 %collective-permute-start.1 = (bf16[256,384]{1,0:T(8,128)(2,1)S(1)}, bf16[256,384]{1,0:T(8,128)(2,1)S(1)}, u32[]{:S(2)}, u32[]{:S(2)}) collective-permute-start(bf16[256,384]{1,0:T(8,128)(2,1)S(1)} %collective-permute-done), channel_id=1, source_target_pairs={{0,8},{4,12},{8,0},{12,4},{16,24},{20,28},{24,16},{28,20},{1,9},{5... | collective-permute-start | bytes 589832 | tf_op jit(solution)/shard_map/ppermute | solution.py:16
  45.1 18.8 %collective-permute-start.2 = (bf16[256,384]{1,0:T(8,128)(2,1)S(1)}, bf16[256,384]{1,0:T(8,128)(2,1)S(1)}, u32[]{:S(2)}, u32[]{:S(2)}) collective-permute-start(bf16[256,384]{1,0:T(8,128)(2,1)S(1)} %collective-permute-done.1), channel_id=1, source_target_pairs={{0,16},{4,20},{8,24},{12,28},{16,0},{20,4},{24,8},{28,12},{1,17},{... | collective-permute-start | bytes 589832 | tf_op jit(solution)/shard_map/ppermute | solution.py:16
  101.5 3.4 copy-start.10
  101.5 3.5 copy-start.8
  209.8 4.1 copy-start.9
  209.8 4.3 copy-start.11
  213.4 22.6 %copy-start.3 = (bf16[128,2048]{1,0:T(8,128)(2,1)S(1)}, bf16[128,2048]{1,0:T(8,128)(2,1)}, u32[]{:S(2)}) copy-start(bf16[128,2048]{1,0:T(8,128)(2,1)} %param.44) | copy-start | bytes 1572868
  214.2 6.5 %collective-permute-start.3 = (bf16[256,384]{0,1:T(8,128)(2,1)S(1)}, bf16[256,384]{0,1:T(8,128)(2,1)S(1)}, u32[]{:S(2)}, u32[]{:S(2)}) collective-permute-start(bf16[256,384]{0,1:T(8,128)(2,1)S(1)} %pad_maximum_fusion.1), channel_id=1, source_target_pairs={{0,4},{4,0},{8,12},{12,8},{16,20},{20,16},{24,28},{28,24},{1,5},{5... | collective-permute-start | bytes 589832 | tf_op jit(solution)/shard_map/ppermute | solution.py:16
  220.7 5.7 collective-permute-start.4
  226.4 9.6 %collective-permute-start.5 = (bf16[256,384]{0,1:T(8,128)(2,1)S(1)}, bf16[256,384]{0,1:T(8,128)(2,1)S(1)}, u32[]{:S(2)}, u32[]{:S(2)}) collective-permute-start(bf16[256,384]{0,1:T(8,128)(2,1)S(1)} %collective-permute-done.4), channel_id=1, source_target_pairs={{0,16},{4,20},{8,24},{12,28},{16,0},{20,4},{24,8},{28,12},{1,17},{... | collective-permute-start | bytes 589832 | tf_op jit(solution)/shard_map/ppermute | solution.py:16
  236.7 32.7 %copy-start.1 = (bf16[128,2048]{1,0:T(8,128)(2,1)S(1)}, bf16[128,2048]{1,0:T(8,128)(2,1)}, u32[]{:S(2)}) copy-start(bf16[128,2048]{1,0:T(8,128)(2,1)} %param.32) | copy-start | bytes 1572868
  236.8 34.0 %copy-start.7 = (f32[2048]{0:T(1024)S(1)}, f32[2048]{0:T(1024)}, u32[]{:S(2)}) copy-start(f32[2048]{0:T(1024)} %param.45) | copy-start | bytes 24580
  238.9 56.6 %all-gather.13.cloned.1.call-start = ((), (), s32[]{:S(2)}) async-start(), calls=%async_computation.7 | async-start | bytes 2621440 | tf_op jit(solution)/shard_map/all_gather | solution.py:192
  272.8 149.2 %all-gather.15.cloned.1.call-start = ((), (), s32[]{:S(2)}) async-start(), calls=%async_computation.8 | async-start | bytes 9437184 | tf_op jit(solution)/shard_map/all_gather | solution.py:195
  273.4 273.8 %all-gather.17.cloned.1.call-start = ((), (), s32[]{:S(2)}) async-start(), calls=%async_computation.9 | async-start | bytes 9437184 | tf_op jit(solution)/shard_map/all_gather | solution.py:199
  274.1 319.1 %copy-start.2 = (bf16[128,2048]{1,0:T(8,128)(2,1)S(1)}, bf16[128,2048]{1,0:T(8,128)(2,1)}, u32[]{:S(2)}) copy-start(bf16[128,2048]{1,0:T(8,128)(2,1)} %reduce-scatter.3.cloned.1.call-done) | copy-start | bytes 1572868
  274.1 319.1 %reduce-scatter.5.cloned.1.call-start = ((), (), s32[]{:S(2)}) async-start(), calls=%async_computation.10 | async-start | bytes 2621440 | tf_op jit(solution)/shard_map/reduce_scatter | solution.py:200
Sparse Core Ops, SparseCore 0:
  9.4 58.5 all-gather.10
  70.0 50.4 all-gather.6
  122.5 48.5 all-gather.8
  239.0 30.3 reduce-scatter.2
  272.9 22.5 all-gather.12
  297.5 124.4 all-gather.14
  424.0 123.1 all-gather.16
  563.8 29.3 reduce-scatter.4
